TPU v7x, 32 devices: a whole 2x2x4 slice. The times are simulated.
32 devices in a mesh: sp: 8 (over z, core), tp: 4 (over y, x).
Axes of the slice: x: 2, y: 2, z: 4, core: 2. Of those that a mesh axis runs over, the one named last changes fastest.
Arguments:
- stream: bfloat16 [2048, 1024], P('tp', 'sp')
- values_in: bfloat16 [1024, 1024], P('tp', 'sp'), may hold values from -6 to 6
- in_gate: bfloat16 [1024, 1024], P('tp', 'sp'), may hold values from -6 to 6
- out_gate: bfloat16 [1024, 1024], P('tp', 'sp'), may hold values from -6 to 6
- documents: int32 [1024], P('sp'), may hold values from 0 to 15, never falling along the last dimension, each value on 1 to 256 neighbouring positions
- conv_taps: float32 [3, 1024], P(None, 'tp'), may hold values from -3.5 to 3.5
- head_gain: float32 [1024], P('tp'), may hold values from 0.1 to 1.9
- mix_weight: bfloat16 [1024, 2048], P('tp'), may hold values from -0.25 to 0.25
- norm_gain: float32 [2048], P('tp'), may hold values from 0.1 to 1.9
- routes: int32 [1024, 4], P('sp'), may hold values from 0 to 7, all different within a row; in each aligned block of 128 rows (0 to 127, 128 to 255, ...) at most 96 rows name the same one
- route_weight: float32 [1024, 4], P('sp'), may hold values from 0.2 to 1
- expert_gate: bfloat16 [8, 2048, 2048], P('sp', None, 'tp'), may hold values from -0.125 to 0.125
- expert_up: bfloat16 [8, 2048, 2048], P('sp', None, 'tp'), may hold values from -0.125 to 0.125
- expert_down: bfloat16 [8, 2048, 2048], P('sp', None, 'tp'), may hold values from -0.125 to 0.125
- shared_gate: bfloat16 [2048, 2048], P(None, 'tp'), may hold values from -0.125 to 0.125
- shared_up: bfloat16 [2048, 2048], P(None, 'tp'), may hold values from -0.125 to 0.125
- shared_down: bfloat16 [2048, 2048], P('tp'), may hold values from -0.1875 to 0.1875
Outputs:
- layer_out: bfloat16 [2048, 1024], P('tp', 'sp')
Inputs may be any that keep to these rules, and one draw needn't show every extreme that they name: `routes`: each row names 4 different experts. In each aligned block of 128 rows no expert is named by more than 96 rows, a bound that some block reaches. `documents`: document numbers never fall along the positions; each document has 1 to 256 positions, and one has exactly that many.
All inputs are finite; a program needn't handle non-finite values.
Results may differ from a plain program's by a relative error of at most 0.015.
Values may be sent and summed in bfloat16 or wider, within the bound.
A program may use at most 64 MiB of HBM per device.

v0:
```python
import jax
import jax.numpy as jnp
from jax import lax
from jax.sharding import PartitionSpec as P

D = 2048
HEAD = 64


epsilon = 1e-06


def from_behind(x, axis, by):
    size = lax.axis_size(axis)
    pairs = [(i, i + by) for i in range(size) if 0 <= i + by < size]
    return lax.ppermute(x, axis, pairs)


def contract_rows(left, right):
    return lax.dot_general(
        left, right, (((0,), (0,)), ((), ())), preferred_element_type=jnp.float32
    )


def local(
    stream,
    values_in,
    in_gate,
    out_gate,
    documents,
    conv_taps,
    head_gain,
    mix_weight,
    norm_gain,
    routes,
    route_weight,
    expert_gate,
    expert_up,
    expert_down,
    shared_gate,
    shared_up,
    shared_down,
):
    positions = stream.shape[1]
    feat_rows = stream.shape[0]
    sp_count = lax.axis_size("sp")
    top_count = routes.shape[1]
    capacity = 3 * positions * top_count // (2 * sp_count)
    slot_total = sp_count * capacity
    tails = jnp.stack([values_in[:, -2:], in_gate[:, -2:]])
    before, before_docs = from_behind((tails, documents[-2:]), "sp", 1)
    joined = jnp.concatenate([before, jnp.stack([values_in, in_gate])], axis=2).astype(jnp.float32)
    product = joined[0] * joined[1]
    doc_ids = jnp.concatenate([before_docs, documents])
    convolved = jnp.zeros((values_in.shape[0], positions), jnp.float32)
    for offset in range(3):
        same_doc = (doc_ids[offset : offset + positions] == documents).astype(jnp.float32)
        convolved = (
            convolved
            + conv_taps[offset][:, None]
            * product[:, offset : offset + positions]
            * same_doc[None, :]
        )
    mixed = out_gate.astype(jnp.float32) * convolved
    heads = mixed.reshape(-1, HEAD, positions)
    heads = heads * lax.rsqrt(jnp.mean(heads * heads, axis=1, keepdims=True) + epsilon)
    normed_heads = (heads.reshape(mixed.shape) * head_gain[:, None]).astype(jnp.bfloat16)
    mixer = lax.psum_scatter(
        contract_rows(mix_weight, normed_heads).astype(jnp.bfloat16),
        "tp",
        scatter_dimension=0,
        tiled=True,
    ).astype(jnp.float32)
    hidden_state = stream.astype(jnp.float32) + mixer
    squares = lax.psum(jnp.sum(hidden_state * hidden_state, axis=0), "tp")
    normed = (hidden_state * lax.rsqrt(squares / D + epsilon)[None, :] * norm_gain[:, None]).astype(
        jnp.bfloat16
    )
    full_rows = lax.all_gather(normed, "tp", axis=0, tiled=True)
    shared_mid = (
        jax.nn.silu(contract_rows(shared_gate, full_rows)) * contract_rows(shared_up, full_rows)
    ).astype(jnp.bfloat16)
    shared = lax.psum_scatter(
        contract_rows(shared_down, shared_mid).astype(jnp.bfloat16),
        "tp",
        scatter_dimension=0,
        tiled=True,
    ).astype(jnp.float32)
    flat_routes = routes.reshape(-1)
    onehot = (flat_routes[:, None] == jnp.arange(sp_count, dtype=jnp.int32)[None, :]).astype(
        jnp.int32
    )
    earlier = jnp.cumsum(onehot, axis=0) - onehot
    slot = jnp.sum(earlier * onehot, axis=1)
    column = flat_routes * capacity + slot
    chosen = (column[:, None] == jnp.arange(slot_total, dtype=jnp.int32)[None, :]).reshape(
        positions, top_count, slot_total
    )
    dispatch = jnp.any(chosen, axis=1).astype(jnp.bfloat16)
    combine = jnp.sum(chosen.astype(jnp.float32) * route_weight[:, :, None], axis=1)
    sent = jnp.dot(normed, dispatch, preferred_element_type=jnp.float32).astype(jnp.bfloat16)
    arrived = lax.all_to_all(
        sent.reshape(feat_rows, sp_count, capacity), "sp", split_axis=1, concat_axis=1, tiled=True
    )
    block_rows = lax.all_gather(arrived.reshape(feat_rows, slot_total), "tp", axis=0, tiled=True)
    gate_rows = expert_gate[0]
    up_rows = expert_up[0]
    gate = contract_rows(gate_rows, block_rows)
    upward = contract_rows(up_rows, block_rows)
    expert_mid = (jax.nn.silu(gate) * upward).astype(jnp.bfloat16)
    weight_rows = expert_down[0]
    summed = contract_rows(
        weight_rows, lax.all_gather(expert_mid, "tp", axis=0, tiled=True)
    ).astype(jnp.bfloat16)
    returned = lax.all_to_all(
        summed.reshape(feat_rows, sp_count, capacity), "sp", split_axis=1, concat_axis=1, tiled=True
    )
    routed = lax.dot_general(
        returned.reshape(feat_rows, slot_total).astype(jnp.float32),
        combine,
        (((1,), (1,)), ((), ())),
        precision=lax.Precision.HIGHEST,
        preferred_element_type=jnp.float32,
    )
    return (hidden_state + shared + routed).astype(jnp.bfloat16)


def solution(mesh):
    in_specs = (
        P("tp", "sp"),
        P("tp", "sp"),
        P("tp", "sp"),
        P("tp", "sp"),
        P("sp"),
        P(None, "tp"),
        P("tp"),
        P("tp", None),
        P("tp"),
        P("sp", None),
        P("sp", None),
        P("sp", None, "tp"),
        P("sp", None, "tp"),
        P("sp", None, "tp"),
        P(None, "tp"),
        P(None, "tp"),
        P("tp", None),
    )
    out_specs = P("tp", "sp")
    return jax.shard_map(local, mesh=mesh, in_specs=in_specs, out_specs=out_specs, check_vma=False)
```

profile of v0, /device:TPU:0, one launch (start us, length us, event | category | flops | bytes accessed | tf_op | source)
XLA Modules:
  0.0 227.8 jit_solution(12113841220716152108)
XLA Ops:
  6.6 0.9 slice.51
  7.5 2.5 %collective-permute-start.1 = (s32[2]{0:T(128)S(1)}, s32[2]{0:T(128)S(1)}, u32[]{:S(2)}, u32[]{:S(2)}) collective-permute-start(s32[2]{0:T(128)S(1)} %slice.51), channel_id=1, source_target_pairs={{0,4},{4,8},{8,12},{12,16},{16,20},{20,24},{24,28},{1,5},{5,9},{9,... | collective-permute-start | bytes 32 | tf_op jit(solution)/shard_map/ppermute | solution.py:16
  10.0 0.9 slice.46
  11.0 0.9 slice.47
  12.1 4.6 %collective-permute-start = (bf16[2,256,2]{1,2,0:T(2,128)(2,1)S(1)}, bf16[2,256,2]{1,2,0:T(2,128)(2,1)S(1)}, u32[]{:S(2)}, u32[]{:S(2)}) collective-permute-start(bf16[2,256,2]{1,2,0:T(2,128)(2,1)S(1)} %pad_maximum_fusion), channel_id=1, source_target_pairs={{0,4},{4,8},{8,12},{12,16},{16,20},{20,24},{24,28},{1,5},{5,9},{9,... | collective-permute-start | bytes 6152 | tf_op jit(solution)/shard_map/ppermute | solution.py:16
  16.7 0.8 fusion.40
  17.5 0.7 pad_add_fusion
  18.2 0.7 compare_convert_fusion.1
  19.1 1.0 maximum_convert_fusion
  20.6 1.1 fusion.1
  22.3 1.1 reduce-window.6
  24.0 0.3 fusion.12
  24.3 23.0 %reduce-scatter.3.cloned.1.call-done = bf16[512,128]{0,1:T(8,128)(2,1)} async-done(((bf16[2048,128]{0,1:T(8,128)(2,1)}), bf16[512,128]{0,1:T(8,128)(2,1)}) %reduce-scatter.3.cloned.1.call-update) | async-done | bytes 131088 | tf_op jit(solution)/shard_map/reduce_scatter | solution.py:68
  47.3 1.0 multiply_reduce_fusion
  48.4 9.0 %psum.7 = f32[128]{0:T(128)S(1)} all-reduce(f32[128]{0:T(128)S(1)} %multiply_reduce_fusion), channel_id=1, replica_groups=mesh['sp'=8,'tp'=4] {'tp'}, use_global_device_ids=true, to_apply=%region_3.0 | all-reduce | flops 128 | bytes 1024 | tf_op jit(solution)/shard_map/psum | solution.py:75
  57.3 1.0 multiply_convert_fusion
  58.3 0.6 copy-done.1
  59.0 1.3 convolution_convert_fusion.2
  60.2 1.4 copy.63
  61.7 25.4 %all_to_all.10 = bf16[512,8,96]{0,2,1:T(8,128)(2,1)} all-to-all(bf16[512,8,96]{0,2,1:T(8,128)(2,1)S(1)} %bitcast.90), channel_id=1, replica_groups=mesh['sp'=8,'tp'=4] {'sp'}, dimensions={1} | all-to-all | bytes 1572864 | tf_op jit(solution)/shard_map/all_to_all | solution.py:102
  87.2 41.8 %all-gather.3.cloned.1.call-done = bf16[2048,768]{0,1:T(8,128)(2,1)} async-done(((bf16[512,768]{0,1:T(8,128)(2,1)}), bf16[2048,768]{0,1:T(8,128)(2,1)}) %all-gather.3.cloned.1.call-update) | async-done | bytes 3145744 | tf_op jit(solution)/shard_map/all_gather | solution.py:105
  129.0 3.8 %fusion.6 = f32[768,512]{1,0:T(8,128)S(1)} fusion(bf16[2048,768]{0,1:T(8,128)(2,1)} %all-gather.3.cloned.1.call-done, bf16[1,2048,512]{2,1,0:T(8,128)(2,1)S(1)} %copy-done), kind=kOutput, calls=%fused_computation.8 | convolution fusion | flops 1610612736 | bytes 6815744 | tf_op jit(solution)/shard_map/dot_general | solution.py:20
  132.8 2.8 %fusion.8 = bf16[512,768]{0,1:T(8,128)(2,1)} fusion(f32[768,512]{1,0:T(8,128)S(1)} %fusion.6, bf16[2048,768]{0,1:T(8,128)(2,1)S(1)} %copy-done.10, bf16[1,2048,512]{2,1,0:T(8,128)(2,1)S(1)} %copy-done.11), kind=kOutput, calls=%fused_computation.11 | convolution fusion | flops 1612972032 | bytes 7602176 | tf_op jit(solution)/shard_map/dot_general | solution.py:20
  135.7 10.1 %all_gather.9 = bf16[2048,128]{0,1:T(8,128)(2,1)S(1)} all-gather(bf16[512,128]{0,1:T(8,128)(2,1)S(1)} %copy-done.2), channel_id=1, replica_groups=mesh['sp'=8,'tp'=4] {'tp'}, dimensions={0}, use_global_device_ids=true | all-gather | bytes 655360 | tf_op jit(solution)/shard_map/all_gather | solution.py:79
  145.8 2.8 %convolution_bitcast_fusion.1 = f32[512,128]{0,1:T(8,128)} fusion(bf16[2048,128]{0,1:T(8,128)(2,1)S(1)} %all_gather.9, bf16[2048,512]{1,0:T(8,128)(2,1)} %param.31), kind=kOutput, calls=%fused_computation.24 | convolution fusion | flops 268435456 | bytes 2883584 | tf_op jit(solution)/shard_map/dot_general | solution.py:20
  148.5 31.0 %all-gather.5.cloned.1.call-done = bf16[2048,768]{0,1:T(8,128)(2,1)} async-done(((bf16[512,768]{0,1:T(8,128)(2,1)}), bf16[2048,768]{0,1:T(8,128)(2,1)}) %all-gather.5.cloned.1.call-update) | async-done | bytes 3145744 | tf_op jit(solution)/shard_map/all_gather | solution.py:113
  179.5 5.2 %fusion.15 = bf16[768,512]{1,0:T(8,128)(2,1)} fusion(bf16[2048,768]{0,1:T(8,128)(2,1)} %all-gather.5.cloned.1.call-done, bf16[1,2048,512]{2,1,0:T(8,128)(2,1)} %param.30), kind=kOutput, calls=%fused_computation.20 | convolution fusion | flops 1611005952 | bytes 6029312 | tf_op jit(solution)/shard_map/dot_general | solution.py:20
  184.7 4.6 %all-to-all-start.1 = ((bf16[512,8,96]{0,2,1:T(8,128)(2,1)}), bf16[512,8,96]{0,2,1:T(8,128)(2,1)S(1)}, u32[]{:S(2)}, u32[]{:S(2)}) async-start(bf16[512,8,96]{0,2,1:T(8,128)(2,1)} %bitcast.92), calls=%async_computation.3 | async-start | bytes 1572864 | tf_op jit(solution)/shard_map/all_to_all | solution.py:115
  189.4 4.0 %fusion = bf16[2048,128]{0,1:T(8,128)(2,1)} fusion(bf16[512,2048]{1,0:T(8,128)(2,1)} %param.33, bf16[2048,128]{0,1:T(8,128)(2,1)S(1)} %all_gather.9, bf16[2048,512]{1,0:T(8,128)(2,1)} %param.32, f32[512,128]{0,1:T(8,128)} %convolution_bitcast_fusion.1), kind=kOutput, calls=%fused_computation.2 | convolution fusion | flops 537526272 | bytes 5505024 | tf_op jit(solution)/shard_map/dot_general | solution.py:20
  193.6 25.5 %reduce-scatter.5.cloned.1.call-done = bf16[512,128]{0,1:T(8,128)(2,1)} async-done(((bf16[2048,128]{0,1:T(8,128)(2,1)}), bf16[512,128]{0,1:T(8,128)(2,1)}) %reduce-scatter.5.cloned.1.call-update) | async-done | bytes 131088 | tf_op jit(solution)/shard_map/reduce_scatter | solution.py:83
  219.1 1.4 fusion.20
  220.6 0.8 copy.65
  (56 shorter events, 2.2 us)
Async XLA Ops:
  6.5 122.4 %copy-start = (bf16[1,2048,512]{2,1,0:T(8,128)(2,1)S(1)}, bf16[1,2048,512]{2,1,0:T(8,128)(2,1)}, u32[]{:S(2)}) copy-start(bf16[1,2048,512]{2,1,0:T(8,128)(2,1)} %param.28) | copy-start | bytes 6291460
  6.5 13.7 %copy-start.5 = (bf16[256,128]{1,0:T(8,128)(2,1)S(1)}, bf16[256,128]{1,0:T(8,128)(2,1)}, u32[]{:S(2)}) copy-start(bf16[256,128]{1,0:T(8,128)(2,1)} %param.20) | copy-start | bytes 196612
  6.5 13.9 %copy-start.9 = (f32[256]{0:T(256)S(1)}, f32[256]{0:T(256)}, u32[]{:S(2)}) copy-start(f32[256]{0:T(256)} %param.23) | copy-start | bytes 3076
  6.5 14.1 %copy-start.3 = (bf16[256,2048]{1,0:T(8,128)(2,1)S(1)}, bf16[256,2048]{1,0:T(8,128)(2,1)}, u32[]{:S(2)}) copy-start(bf16[256,2048]{1,0:T(8,128)(2,1)} %param.24) | copy-start | bytes 3145732
  6.5 40.8 %reduce-scatter.3.cloned.1.call-start = ((), (), s32[]{:S(2)}) async-start(), calls=%async_computation.4 | async-start | bytes 655360 | tf_op jit(solution)/shard_map/reduce_scatter | solution.py:68
  7.5 10.0 %collective-permute-start.1 = (s32[2]{0:T(128)S(1)}, s32[2]{0:T(128)S(1)}, u32[]{:S(2)}, u32[]{:S(2)}) collective-permute-start(s32[2]{0:T(128)S(1)} %slice.51), channel_id=1, source_target_pairs={{0,4},{4,8},{8,12},{12,16},{16,20},{20,24},{24,28},{1,5},{5,9},{9,... | collective-permute-start | bytes 32 | tf_op jit(solution)/shard_map/ppermute | solution.py:16
  12.1 6.9 %collective-permute-start = (bf16[2,256,2]{1,2,0:T(2,128)(2,1)S(1)}, bf16[2,256,2]{1,2,0:T(2,128)(2,1)S(1)}, u32[]{:S(2)}, u32[]{:S(2)}) collective-permute-start(bf16[2,256,2]{1,2,0:T(2,128)(2,1)S(1)} %pad_maximum_fusion), channel_id=1, source_target_pairs={{0,4},{4,8},{8,12},{12,16},{16,20},{20,24},{24,28},{1,5},{5,9},{9,... | collective-permute-start | bytes 6152 | tf_op jit(solution)/shard_map/ppermute | solution.py:16
  19.1 2.7 %copy-start.6 = (s32[128,4]{0,1:T(4,128)S(1)}, s32[128,4]{0,1:T(4,128)}, u32[]{:S(2)}) copy-start(s32[128,4]{0,1:T(4,128)} %param.26) | copy-start | bytes 6148
  20.1 2.0 copy-start.4
  20.2 37.1 %copy-start.7 = (f32[512]{0:T(512)S(1)}, f32[512]{0:T(512)}, u32[]{:S(2)}) copy-start(f32[512]{0:T(512)} %param.25) | copy-start | bytes 6148
  21.8 107.2 %all-gather.3.cloned.1.call-start = ((), (), s32[]{:S(2)}) async-start(), calls=%async_computation.6 | async-start | bytes 3932160 | tf_op jit(solution)/shard_map/all_gather | solution.py:105
  58.3 0.7 copy-start.1
  87.1 92.4 %all-gather.5.cloned.1.call-start = ((), (), s32[]{:S(2)}) async-start(), calls=%async_computation.7 | async-start | bytes 3932160 | tf_op jit(solution)/shard_map/all_gather | solution.py:113
  129.0 3.8 %copy-start.10 = (bf16[2048,768]{0,1:T(8,128)(2,1)S(1)}, bf16[2048,768]{0,1:T(8,128)(2,1)}, u32[]{:S(2)}) copy-start(bf16[2048,768]{0,1:T(8,128)(2,1)} %all-gather.3.cloned.1.call-done) | copy-start | bytes 9437188
  129.0 3.8 %copy-start.11 = (bf16[1,2048,512]{2,1,0:T(8,128)(2,1)S(1)}, bf16[1,2048,512]{2,1,0:T(8,128)(2,1)}, u32[]{:S(2)}) copy-start(bf16[1,2048,512]{2,1,0:T(8,128)(2,1)} %param.29) | copy-start | bytes 6291460
  132.8 2.9 %copy-start.2 = (bf16[512,128]{0,1:T(8,128)(2,1)S(1)}, bf16[512,128]{0,1:T(8,128)(2,1)}, u32[]{:S(2)}) copy-start(bf16[512,128]{0,1:T(8,128)(2,1)} %copy-done.1) | copy-start | bytes 393220
  184.7 34.3 %all-to-all-start.1 = ((bf16[512,8,96]{0,2,1:T(8,128)(2,1)}), bf16[512,8,96]{0,2,1:T(8,128)(2,1)S(1)}, u32[]{:S(2)}, u32[]{:S(2)}) async-start(bf16[512,8,96]{0,2,1:T(8,128)(2,1)} %bitcast.92), calls=%async_computation.3 | async-start | bytes 1572864 | tf_op jit(solution)/shard_map/all_to_all | solution.py:115
  189.4 4.0 %copy-start.8 = (f32[128,4]{0,1:T(4,128)S(1)}, f32[128,4]{0,1:T(4,128)}, u32[]{:S(2)}) copy-start(f32[128,4]{0,1:T(4,128)} %param.27) | copy-start | bytes 6148
  189.4 29.7 %reduce-scatter.5.cloned.1.call-start = ((), (), s32[]{:S(2)}) async-start(), calls=%async_computation.5 | async-start | bytes 655360 | tf_op jit(solution)/shard_map/reduce_scatter | solution.py:83
Sparse Core Ops, SparseCore 0:
  21.9 25.3 reduce-scatter.2
  87.2 41.6 all-gather.2
  135.8 43.7 all-gather.4
  193.5 25.5 reduce-scatter.4
where the time goes:
time: 228 us
  waiting for transfers between devices  121 us (53%)
  blocking collectives  44.5 us (20%)
  matrix products  22.4 us (10%)
  between operations  13.4 us (6%)
  starting transfers between devices  11.9 us (5%)
  local copies, waits for them, and re-layouts  7.61 us (3%)
  other arithmetic  6.72 us (3%)
    all_gather x1, waiting for transfers between devices, local(): lax.all_gather(arrived.reshape(feat_rows, slot_total), 'tp', axis=0, tile...  41.8 us
    all_gather x1, waiting for transfers between devices, local(): lax.all_gather(expert_mid, 'tp', axis=0, tiled=True)  31 us
    reduce_scatter x1, waiting for transfers between devices, local(): lax.psum_scatter(contract_rows(shared_down, shared_mid).astype(jnp.bfloat...  25.5 us
    all_to_all x1, blocking collectives, local(): lax.all_to_all(sent.reshape(feat_rows, sp_count, capacity), 'sp', split_a...  25.4 us
    reduce_scatter x1, waiting for transfers between devices, local(): lax.psum_scatter(contract_rows(mix_weight, normed_heads).astype(jnp.bfloa...  23 us
    dot_general x6, matrix products, contract_rows(): lax.dot_general(left, right, (((0,), (0,)), ((), ())), preferred_element_...  19.7 us
    all_gather x1, blocking collectives, local(): full_rows = lax.all_gather(normed, 'tp', axis=0, tiled=True)  10.1 us
    psum x1, blocking collectives, local(): squares = lax.psum(jnp.sum(hidden_state * hidden_state, axis=0), 'tp')  8.96 us
  transfers between devices with their start and end apart: 7, of which 4 were waited for; matrix products, arithmetic and copies ran while one was open for 6% of the time, Pallas kernels for 0%

commit v1 on v0

v1 whole, which is shorter than its diff:
```python
import functools

import jax
import jax.numpy as jnp
from jax import lax
from jax.experimental import pallas as pl
from jax.experimental.pallas import tpu as pltpu
from jax.sharding import PartitionSpec as P

HEAD = 64
CORES = 2
CHUNKS = 4
SUB = 8
epsilon = 1e-06
MESH = pl.DeviceIdType.MESH
F32 = jnp.float32
BF16 = jnp.bfloat16


def flipped(index, mask):
    bit = 1
    out = index
    while bit <= mask:
        if mask & bit:
            out = out + bit - 2 * bit * lax.rem(lax.div(index, bit), 2)
        bit *= 2
    return out


def dot(left, right):
    return jnp.dot(left, right, preferred_element_type=F32)


def silu(value):
    return value / (1.0 + jnp.exp(-value))


def column_of(row, width):
    return jnp.broadcast_to(row, (width, row.shape[1])).T


def kernel(
    n_sp, n_tp,
    stream, values_in, in_gate, out_gate, documents, conv_taps, head_gain, mix_weight,
    norm_gain, routes, route_weight, expert_gate, expert_up, expert_down,
    shared_gate, shared_up, shared_down,
    out,
    mix_w, gate_w, up_w, sgate_w, sup_w, sdown_w, down_w,
    tail_s, prev_r, prev_docs, mix_s, mix_r, hidden_v, x_all, ss_s, ss_r, meta_r,
    mid_v, shared_v, acc_v, pr_s, pr_r, rs_s, rs_r, zr_s, zr_r,
    load_sem, local_sem, halo_send, halo_recv, mix_send, mix_recv, ss_send, ss_recv,
    meta_send, meta_recv, x_recv, xs_tp, xs_z, xs_p, wd_send, wd_recv,
    pr_send, pr_recv, rs_send, rs_recv, zr_send, zr_recv,
):
    sp = lax.axis_index("sp")
    tp = lax.axis_index("tp")
    z = lax.div(sp, CORES)
    core = lax.rem(sp, CORES)
    n_z = n_sp // CORES
    feats, pos = stream.shape
    chans = values_in.shape[0]
    width = feats * n_tp
    hid = gate_w.shape[1]
    partner = {"sp": z * CORES + 1 - core}
    peers = [flipped(tp, d) for d in range(1, n_tp)]
    pending = []

    def send(src, dst, ssem, rsem, device):
        copy = pltpu.make_async_remote_copy(
            src_ref=src, dst_ref=dst, send_sem=ssem, recv_sem=rsem,
            device_id=device, device_id_type=MESH,
        )
        copy.start()
        pending.append(copy)

    def arrived(dst, rsem):
        pltpu.make_async_remote_copy(
            src_ref=dst, dst_ref=dst, send_sem=rsem, recv_sem=rsem,
            device_id=partner, device_id_type=MESH,
        ).wait_recv()

    loads = [
        pltpu.make_async_copy(src, dst, load_sem.at[i])
        for i, (src, dst) in enumerate([
            (mix_weight, mix_w), (shared_gate, sgate_w), (shared_up, sup_w),
            (shared_down, sdown_w), (expert_gate.at[0], gate_w), (expert_up.at[0], up_w),
        ])
    ]
    loads[0].start()

    barrier = pltpu.get_barrier_semaphore()
    for peer in peers:
        pl.semaphore_signal(barrier, inc=1, device_id={"tp": peer}, device_id_type=MESH)
    for d in range(1, n_sp):
        pl.semaphore_signal(
            barrier, inc=1, device_id={"sp": lax.rem(sp + d, n_sp)}, device_id_type=MESH
        )
    pl.semaphore_wait(barrier, n_tp - 1 + n_sp - 1)

    product = values_in[...].astype(F32) * in_gate[...].astype(F32)
    tail_s[...] = product.T[pos - SUB:, :]
    after = {"sp": lax.rem(sp + 1, n_sp)}
    send(tail_s, prev_r.at[pl.ds(pos - SUB, SUB)], halo_send.at[0], halo_recv.at[0], after)
    send(documents, prev_docs, halo_send.at[1], halo_recv.at[1], after)

    rows = hid // CHUNKS

    def send_down(chunk):
        for d, peer in enumerate(peers):
            start = pl.multiple_of(peer * hid + chunk * rows, rows)
            send(
                expert_down.at[0, pl.ds(start, rows), :],
                down_w.at[tp, pl.ds(chunk * rows, rows), :],
                wd_send.at[d, chunk], wd_recv.at[tp, chunk], {"tp": peer},
            )

    send_down(0)
    own_down = pltpu.make_async_copy(
        expert_down.at[0, pl.ds(pl.multiple_of(tp * hid, hid), hid), :], down_w.at[tp], local_sem
    )
    for load in loads[1:]:
        load.start()
    own_down.start()

    named = routes[...]
    weights = route_weight[...]
    meta_rows = meta_r.shape[1]
    lane = lax.broadcasted_iota(jnp.int32, (pos, pos), 1)
    table = jnp.zeros((pos, pos), F32)
    for k in range(routes.shape[1]):
        table = table + jnp.where(lane == named[:, k:k + 1], weights[:, k:k + 1], 0.0)
    table = table.T[:meta_rows]
    taps = [column_of(conv_taps[j:j + 1, :], pos) for j in range(3)]
    stream_t = stream[...].astype(F32).T

    prev_r[: pos - SUB, :] = jnp.zeros((pos - SUB, chans), F32)
    arrived(prev_r.at[pl.ds(pos - SUB, SUB)], halo_recv.at[0])
    arrived(prev_docs, halo_recv.at[1])
    before = prev_r[...].T
    docs = documents[...]
    docs_before = jnp.where(sp > 0, prev_docs[...], -1)
    lane_c = lax.broadcasted_iota(jnp.int32, (chans, pos), 1)
    lane_1 = lax.broadcasted_iota(jnp.int32, (1, pos), 1)
    convolved = taps[2] * product
    for shift in (1, 2):
        moved = jnp.where(lane_c < shift, pltpu.roll(before, shift, 1), pltpu.roll(product, shift, 1))
        ids = jnp.where(lane_1 < shift, pltpu.roll(docs_before, shift, 1), pltpu.roll(docs, shift, 1))
        convolved = convolved + jnp.where(ids == docs, taps[2 - shift] * moved, 0.0)
    mixed = out_gate[...].astype(F32) * convolved
    heads = mixed.reshape(chans // HEAD, HEAD, pos)
    heads = heads * lax.rsqrt(jnp.mean(heads * heads, axis=1, keepdims=True) + epsilon)
    heads_t = (heads.reshape(chans, pos).T * head_gain[...]).astype(BF16)

    loads[0].wait()
    for b, peer in enumerate(peers + [tp]):
        cols = pl.ds(pl.multiple_of(peer * feats, feats), feats)
        mix_s[b] = dot(heads_t, mix_w[:, cols]).astype(BF16)
        if b < n_tp - 1:
            send(mix_s.at[b], mix_r.at[b], mix_send.at[b], mix_recv.at[b], {"tp": peer})
    send_down(1)

    hidden = stream_t + mix_s[n_tp - 1].astype(F32)
    for b in range(n_tp - 1):
        arrived(mix_r.at[b], mix_recv.at[b])
        hidden = hidden + mix_r[b].astype(F32)
    hidden_v[...] = hidden
    x_all[sp, tp] = (hidden * norm_gain[...]).astype(BF16)
    own = x_all.at[sp, tp]
    for d in range(1, n_z):
        send(own, own, xs_z.at[d], x_recv.at[sp, tp],
             {"sp": lax.rem(z + d, n_z) * CORES + core})
    for b, peer in enumerate(peers):
        send(own, own, xs_tp.at[0, b], x_recv.at[sp, tp], {"tp": peer})
    send(own, own, xs_p.at[0, 0], x_recv.at[sp, tp], partner)

    squares = jnp.sum(hidden * hidden, axis=1, keepdims=True)
    row = jnp.broadcast_to(squares, (pos, pos)).T[:SUB]
    ss_s[...] = row
    for b, peer in enumerate(peers):
        send(ss_s, ss_r.at[b], ss_send.at[b], ss_recv.at[b], {"tp": peer})
    send_down(2)
    for b in range(n_tp - 1):
        arrived(ss_r.at[b], ss_recv.at[b])
        row = row + ss_r[b]
    scale = lax.rsqrt(row[:1] / width + epsilon)
    at_row = lax.broadcasted_iota(jnp.int32, (meta_rows, pos), 0)
    meta_r[sp] = jnp.where(at_row == meta_rows - 1, scale, table)
    for d in range(1, n_sp):
        send(meta_r.at[sp], meta_r.at[sp], meta_send.at[d], meta_recv.at[sp],
             {"sp": lax.rem(sp + d, n_sp)})

    def forward(slot, group):
        for b, peer in enumerate(peers):
            block = x_all.at[group, peer]
            arrived(block, x_recv.at[group, peer])
            send(block, block, xs_p.at[slot, b + 1], x_recv.at[group, peer], partner)

    forward(0, sp)

    loads[1].wait()
    loads[2].wait()
    scale_own = column_of(scale, pos)[:, :1]
    gate = jnp.zeros((pos, hid), F32)
    upward = jnp.zeros((pos, hid), F32)
    for b in range(n_tp):
        block = x_all[sp, b]
        gate = gate + dot(block, sgate_w[b * feats:(b + 1) * feats, :])
        upward = upward + dot(block, sup_w[b * feats:(b + 1) * feats, :])
    shared_mid = (silu(gate * scale_own) * (upward * scale_own)).astype(BF16)
    loads[3].wait()
    shared_v[...] = dot(shared_mid, sdown_w[...])

    for d in range(1, n_z):
        group = lax.rem(z + n_z - d, n_z) * CORES + core
        block = x_all.at[group, tp]
        arrived(block, x_recv.at[group, tp])
        for b, peer in enumerate(peers):
            send(block, block, xs_tp.at[d, b], x_recv.at[group, tp], {"tp": peer})
        send(block, block, xs_p.at[d, 0], x_recv.at[group, tp], partner)
    for chunk in range(3, CHUNKS):
        send_down(chunk)

    loads[4].wait()
    loads[5].wait()
    for d in range(n_z):
        layer = lax.rem(z + n_z - d, n_z)
        mine = layer * CORES + core
        other = layer * CORES + 1 - core
        if d > 0:
            forward(d, mine)
            arrived(meta_r.at[mine], meta_recv.at[mine])
        arrived(meta_r.at[other], meta_recv.at[other])
        for b in range(n_tp):
            arrived(x_all.at[other, b], x_recv.at[other, b])
        gate = jnp.zeros((CORES * pos, hid), F32)
        upward = jnp.zeros((CORES * pos, hid), F32)
        for b in range(n_tp):
            block = x_all[pl.ds(layer * CORES, CORES), b].reshape(CORES * pos, feats)
            gate = gate + dot(block, gate_w[b * feats:(b + 1) * feats, :])
            upward = upward + dot(block, up_w[b * feats:(b + 1) * feats, :])
        scales = jnp.concatenate([
            column_of(meta_r[layer * CORES + i, meta_rows - 1:, :], pos)[:, :1]
            for i in range(CORES)
        ], axis=0)
        mid_v[layer] = (silu(gate * scales) * (upward * scales)).astype(BF16)

    own_down.wait()
    for peer in peers:
        for chunk in range(CHUNKS):
            arrived(down_w.at[peer, pl.ds(chunk * rows, rows), :], wd_recv.at[peer, chunk])

    order = list(range(1, n_z)) + [0]
    totals = {}

    def layer_of(step):
        return lax.rem(z + order[step], n_z)

    def multiply(step):
        layer = layer_of(step)
        for half in range(2):
            group = layer * CORES + (1 - core if half == 0 else core)
            weight = column_of(meta_r[group, pl.ds(sp, 1), :], pos)[:, :1]
            start = pl.multiple_of((group - layer * CORES) * pos, pos)
            middle = mid_v[layer, pl.ds(start, pos), :]
            for b in range(n_tp):
                term = dot(middle, down_w[b]) * weight
                if half == 0:
                    pr_s[step, b] = term.astype(BF16)
                else:
                    acc_v[step % 2, b] = term
            if half == 0:
                send(pr_s.at[step], pr_r.at[step], pr_send.at[step], pr_recv.at[step], partner)

    def spread(step):
        arrived(pr_r.at[step], pr_recv.at[step])
        for b, peer in enumerate(peers + [tp]):
            term = acc_v[step % 2, peer] + pr_r[step, peer].astype(F32)
            if order[step] == 0:
                cols = pl.ds(pl.multiple_of(peer * feats, feats), feats)
                term = term + shared_v[:, cols]
            rs_s[step, b] = term.astype(BF16)
            if b < n_tp - 1:
                send(rs_s.at[step, b], rs_r.at[step, b], rs_send.at[step, b],
                     rs_recv.at[step, b], {"tp": peer})

    def gathered(step):
        total = rs_s[step, n_tp - 1].astype(F32)
        for b in range(n_tp - 1):
            arrived(rs_r.at[step, b], rs_recv.at[step, b])
            total = total + rs_r[step, b].astype(F32)
        d = order[step]
        if d == 0:
            totals[0] = total
        else:
            zr_s[d] = total.astype(BF16)
            send(zr_s.at[d], zr_r.at[d], zr_send.at[d], zr_recv.at[d],
                 {"sp": layer_of(step) * CORES + core})

    for step in range(n_z + 2):
        if step < n_z:
            multiply(step)
        if 0 <= step - 1 < n_z:
            spread(step - 1)
        if 0 <= step - 2 < n_z:
            gathered(step - 2)

    result = hidden_v[...] + totals[0]
    for d in range(1, n_z):
        arrived(zr_r.at[d], zr_recv.at[d])
        result = result + zr_r[d].astype(F32)
    out[...] = result.T.astype(BF16)
    for copy in pending:
        copy.wait_send()


def local(n_sp, n_tp, *args):
    (stream, values_in, in_gate, out_gate, documents, conv_taps, head_gain, mix_weight,
     norm_gain, routes, route_weight, expert_gate, expert_up, expert_down,
     shared_gate, shared_up, shared_down) = args
    feats, pos = stream.shape
    chans = values_in.shape[0]
    width = feats * n_tp
    hid = expert_gate.shape[2]
    n_z = n_sp // CORES
    meta_rows = -(-(n_sp + 1) // SUB) * SUB
    vmem = pl.BlockSpec(memory_space=pltpu.VMEM)
    anywhere = pl.BlockSpec(memory_space=pl.ANY)
    dma = pltpu.SemaphoreType.DMA
    scratch = [
        pltpu.VMEM((chans, width), BF16),
        pltpu.VMEM((width, hid), BF16),
        pltpu.VMEM((width, hid), BF16),
        pltpu.VMEM((width, hid), BF16),
        pltpu.VMEM((width, hid), BF16),
        pltpu.VMEM((hid, width), BF16),
        pltpu.VMEM((n_tp, hid, feats), BF16),
        pltpu.VMEM((SUB, chans), F32),
        pltpu.VMEM((pos, chans), F32),
        pltpu.VMEM((1, pos), jnp.int32),
        pltpu.VMEM((n_tp, pos, feats), BF16),
        pltpu.VMEM((n_tp, pos, feats), BF16),
        pltpu.VMEM((pos, feats), F32),
        pltpu.VMEM((n_sp, n_tp, pos, feats), BF16),
        pltpu.VMEM((SUB, pos), F32),
        pltpu.VMEM((n_tp, SUB, pos), F32),
        pltpu.VMEM((n_sp, meta_rows, pos), F32),
        pltpu.VMEM((n_z, CORES * pos, hid), BF16),
        pltpu.VMEM((pos, width), F32),
        pltpu.VMEM((2, n_tp, pos, feats), F32),
        pltpu.VMEM((n_z, n_tp, pos, feats), BF16),
        pltpu.VMEM((n_z, n_tp, pos, feats), BF16),
        pltpu.VMEM((n_z, n_tp, pos, feats), BF16),
        pltpu.VMEM((n_z, n_tp, pos, feats), BF16),
        pltpu.VMEM((n_z, pos, feats), BF16),
        pltpu.VMEM((n_z, pos, feats), BF16),
        dma((6,)), dma,
        dma((2,)), dma((2,)),
        dma((n_tp,)), dma((n_tp,)),
        dma((n_tp,)), dma((n_tp,)),
        dma((n_sp,)), dma((n_sp,)),
        dma((n_sp, n_tp)),
        dma((n_z, n_tp)), dma((n_z,)), dma((n_z, n_tp)),
        dma((n_tp, CHUNKS)), dma((n_tp, CHUNKS)),
        dma((n_z,)), dma((n_z,)),
        dma((n_z, n_tp)), dma((n_z, n_tp)),
        dma((n_z,)), dma((n_z,)),
    ]
    return pl.pallas_call(
        functools.partial(kernel, n_sp, n_tp),
        out_shape=jax.ShapeDtypeStruct((feats, pos), BF16),
        in_specs=[vmem] * 7 + [anywhere] + [vmem] * 3 + [anywhere] * 6,
        out_specs=vmem,
        scratch_shapes=scratch,
        compiler_params=pltpu.CompilerParams(
            collective_id=0, has_side_effects=True, vmem_limit_bytes=64 * 1024 * 1024 - 65536
        ),
    )(
        stream, values_in, in_gate, out_gate, documents.reshape(1, pos), conv_taps,
        head_gain.reshape(1, chans), mix_weight, norm_gain.reshape(1, feats), routes,
        route_weight, expert_gate, expert_up, expert_down, shared_gate, shared_up, shared_down,
    )


def solution(mesh):
    in_specs = (
        P("tp", "sp"),
        P("tp", "sp"),
        P("tp", "sp"),
        P("tp", "sp"),
        P("sp"),
        P(None, "tp"),
        P("tp"),
        P("tp", None),
        P("tp"),
        P("sp", None),
        P("sp", None),
        P("sp", None, "tp"),
        P("sp", None, "tp"),
        P("sp", None, "tp"),
        P(None, "tp"),
        P(None, "tp"),
        P("tp", None),
    )
    body = functools.partial(local, mesh.shape["sp"], mesh.shape["tp"])
    return jax.shard_map(
        body, mesh=mesh, in_specs=in_specs, out_specs=P("tp", "sp"), check_vma=False
    )
```

time: 228 us -> 94.6 us (0.41)
  waiting for transfers between devices: 121 us -> 0 us
  Pallas kernels: 0 us -> 90 us
  blocking collectives: 44.5 us -> 0 us
  matrix products: 22.4 us -> 0 us
  between operations: 13.4 us -> 0.01 us
  starting transfers between devices: 11.9 us -> 0 us
  other arithmetic: 6.72 us -> 0 us
  local copies, waits for them, and re-layouts: 7.61 us -> 4.39 us
    pallas_call x0 -> x1, Pallas kernels: none -> 90 us  [local(): pl.pallas_call(functools.partial(kernel, n_sp, n_tp), out_shape=jax.Shape...]
    all_gather x2 -> x0, waiting for transfers between devices: 72.8 us -> none  [the longest x1 41.8 us: local(): lax.all_gather(arrived.reshape(feat_rows, slot_total), 'tp', axis=0, tile...]
    reduce_scatter x2 -> x0, waiting for transfers between devices: 48.5 us -> none  [the longest x1 25.5 us: local(): lax.psum_scatter(contract_rows(shared_down, shared_mid).astype(jnp.bfloat...]
    all_to_all x1 -> x0, blocking collectives: 25.4 us -> none  [local(): lax.all_to_all(sent.reshape(feat_rows, sp_count, capacity), 'sp', split_a...]
    dot_general x8 -> x0, matrix products: 22.4 us -> none  [the longest x6 19.7 us: contract_rows(): lax.dot_general(left, right, (((0,), (0,)), ((), ())), preferred_element_...]
    all_gather x1 -> x0, blocking collectives: 10.1 us -> none  [local(): full_rows = lax.all_gather(normed, 'tp', axis=0, tiled=True)]
    psum x1 -> x0, blocking collectives: 8.96 us -> none  [local(): squares = lax.psum(jnp.sum(hidden_state * hidden_state, axis=0), 'tp')]
    ppermute x2 -> x0, starting transfers between devices: 7.1 us -> none  [from_behind(): return lax.ppermute(x, axis, pairs)]
  transfers between devices with their start and end apart: 7 -> 0, of which waited for: 4 -> 0; matrix products, arithmetic and copies ran while one was open for 6% -> 0% of each run, Pallas kernels for 0% -> 0%
where the time goes in v1:
time: 94.6 us; the launch traced here: 94.4 us
  Pallas kernels  90 us (95%)
  local copies, waits for them, and re-layouts  4.39 us (5%)
    pallas_call x1, Pallas kernels, local(): pl.pallas_call(functools.partial(kernel, n_sp, n_tp), out_shape=jax.Shape...  90 us
    unnamed x3, local copies, waits for them, and re-layouts  4.39 us

profile of v1, /device:TPU:0, one launch (start us, length us, event | category | flops | bytes accessed | tf_op | source)
XLA Modules:
  0.0 94.4 jit_solution(16660323971147210848)
XLA Ops:
  0.0 1.4 %copy.18.routes = s32[128,4]{1,0:T(8,128)} copy(s32[128,4]{0,1:T(4,128)} %param.26) | data formatting | bytes 4096 | tf_op args[9]
  1.4 1.4 %copy.19.route_weight = f32[128,4]{1,0:T(8,128)} copy(f32[128,4]{0,1:T(4,128)} %param.27) | data formatting | bytes 4096 | tf_op args[10]
  2.8 90.0 %shard_map.163 = bf16[512,128]{1,0:T(8,128)(2,1)} custom-call(bf16[512,128]{1,0:T(8,128)(2,1)} %stream.1, bf16[256,128]{1,0:T(8,128)(2,1)} %values_in.1, bf16[256,128]{1,0:T(8,128)(2,1)} %in_gate.1, bf16[256,128]{1,0:T(8,128)(2,1)} %out_gate.1, s32[1,128]{1,0:T(1,128)} %bitcast.5, f32[3,256]{1,0:T(4,128)} %conv_taps.1, f32[1,256]{1,0:T(1,128)} %bitcast.4, ...), custom_call_target="tpu_custom_call" | custom-call | tf_op jit(solution)/shard_map/pallas_call | solution.py:368
  92.8 1.6 %copy.21 = bf16[512,128]{1,0:T(8,128)(2,1)} copy(bf16[512,128]{1,0:T(8,128)(2,1)} %shard_map.163) | data formatting | bytes 262144

commit v2 on v1

--- a/solution.py
+++ b/solution.py
@@ -9,7 +9,7 @@
 
 HEAD = 64
 CORES = 2
-CHUNKS = 4
+CHUNKS = 8
 SUB = 8
 epsilon = 1e-06
 MESH = pl.DeviceIdType.MESH
@@ -47,9 +47,9 @@
     out,
     mix_w, gate_w, up_w, sgate_w, sup_w, sdown_w, down_w,
     tail_s, prev_r, prev_docs, mix_s, mix_r, hidden_v, x_all, ss_s, ss_r, meta_r,
-    mid_v, shared_v, acc_v, pr_s, pr_r, rs_s, rs_r, zr_s, zr_r,
+    mid_v, shared_v, acc_v, pr_s, pr_r, rs_s, rs_r, rd_r, zr_s, zr_r,
     load_sem, local_sem, halo_send, halo_recv, mix_send, mix_recv, ss_send, ss_recv,
-    meta_send, meta_recv, x_recv, xs_tp, xs_z, xs_p, wd_send, wd_recv,
+    meta_send, meta_recv, x_recv, xs_tp, xs_z, xs_d, xs_p, wd_send, wd_recv,
     pr_send, pr_recv, rs_send, rs_recv, zr_send, zr_recv,
 ):
     sp = lax.axis_index("sp")
@@ -63,6 +63,9 @@
     hid = gate_w.shape[1]
     partner = {"sp": z * CORES + 1 - core}
     peers = [flipped(tp, d) for d in range(1, n_tp)]
+    square = n_tp == 4
+    near = peers[:2] if square else peers
+    layers = [flipped(z, d) for d in range(n_z)]
     pending = []
 
     def send(src, dst, ssem, rsem, device):
@@ -114,7 +117,8 @@
                 wd_send.at[d, chunk], wd_recv.at[tp, chunk], {"tp": peer},
             )
 
-    send_down(0)
+    for chunk in (0, 1):
+        send_down(chunk)
     own_down = pltpu.make_async_copy(
         expert_down.at[0, pl.ds(pl.multiple_of(tp * hid, hid), hid), :], down_w.at[tp], local_sem
     )
@@ -157,7 +161,7 @@
         mix_s[b] = dot(heads_t, mix_w[:, cols]).astype(BF16)
         if b < n_tp - 1:
             send(mix_s.at[b], mix_r.at[b], mix_send.at[b], mix_recv.at[b], {"tp": peer})
-    send_down(1)
+    send_down(2)
 
     hidden = stream_t + mix_s[n_tp - 1].astype(F32)
     for b in range(n_tp - 1):
@@ -167,8 +171,7 @@
     x_all[sp, tp] = (hidden * norm_gain[...]).astype(BF16)
     own = x_all.at[sp, tp]
     for d in range(1, n_z):
-        send(own, own, xs_z.at[d], x_recv.at[sp, tp],
-             {"sp": lax.rem(z + d, n_z) * CORES + core})
+        send(own, own, xs_z.at[d], x_recv.at[sp, tp], {"sp": layers[d] * CORES + core})
     for b, peer in enumerate(peers):
         send(own, own, xs_tp.at[0, b], x_recv.at[sp, tp], {"tp": peer})
     send(own, own, xs_p.at[0, 0], x_recv.at[sp, tp], partner)
@@ -178,7 +181,7 @@
     ss_s[...] = row
     for b, peer in enumerate(peers):
         send(ss_s, ss_r.at[b], ss_send.at[b], ss_recv.at[b], {"tp": peer})
-    send_down(2)
+    send_down(3)
     for b in range(n_tp - 1):
         arrived(ss_r.at[b], ss_recv.at[b])
         row = row + ss_r[b]
@@ -189,13 +192,29 @@
         send(meta_r.at[sp], meta_r.at[sp], meta_send.at[d], meta_recv.at[sp],
              {"sp": lax.rem(sp + d, n_sp)})
 
-    def forward(slot, group):
-        for b, peer in enumerate(peers):
-            block = x_all.at[group, peer]
-            arrived(block, x_recv.at[group, peer])
-            send(block, block, xs_p.at[slot, b + 1], x_recv.at[group, peer], partner)
-
-    forward(0, sp)
+    def to_partner(slot, b, group):
+        block = x_all.at[group, peers[b]]
+        arrived(block, x_recv.at[group, peers[b]])
+        send(block, block, xs_p.at[slot, b + 1], x_recv.at[group, peers[b]], partner)
+
+    def from_layer(d):
+        group = layers[d] * CORES + core
+        block = x_all.at[group, tp]
+        arrived(block, x_recv.at[group, tp])
+        for b, peer in enumerate(near):
+            send(block, block, xs_tp.at[d, b], x_recv.at[group, tp], {"tp": peer})
+        send(block, block, xs_p.at[d, 0], x_recv.at[group, tp], partner)
+
+    for b in range(n_tp - 1):
+        to_partner(0, b, sp)
+    if square:
+        block = x_all.at[sp, peers[2]]
+        for d in range(1, n_z):
+            send(block, block, xs_d.at[d], x_recv.at[sp, peers[2]],
+                 {"sp": layers[d] * CORES + core})
+    from_layer(1)
+    for chunk in (4, 5):
+        send_down(chunk)
 
     loads[1].wait()
     loads[2].wait()
@@ -210,24 +229,20 @@
     loads[3].wait()
     shared_v[...] = dot(shared_mid, sdown_w[...])
 
-    for d in range(1, n_z):
-        group = lax.rem(z + n_z - d, n_z) * CORES + core
-        block = x_all.at[group, tp]
-        arrived(block, x_recv.at[group, tp])
-        for b, peer in enumerate(peers):
-            send(block, block, xs_tp.at[d, b], x_recv.at[group, tp], {"tp": peer})
-        send(block, block, xs_p.at[d, 0], x_recv.at[group, tp], partner)
-    for chunk in range(3, CHUNKS):
+    for d in range(2, n_z):
+        from_layer(d)
+    for chunk in (6, 7):
         send_down(chunk)
 
     loads[4].wait()
     loads[5].wait()
     for d in range(n_z):
-        layer = lax.rem(z + n_z - d, n_z)
+        layer = layers[d]
         mine = layer * CORES + core
         other = layer * CORES + 1 - core
         if d > 0:
-            forward(d, mine)
+            for b in range(n_tp - 1):
+                to_partner(d, b, mine)
             arrived(meta_r.at[mine], meta_recv.at[mine])
         arrived(meta_r.at[other], meta_recv.at[other])
         for b in range(n_tp):
@@ -249,43 +264,61 @@
         for chunk in range(CHUNKS):
             arrived(down_w.at[peer, pl.ds(chunk * rows, rows), :], wd_recv.at[peer, chunk])
 
-    order = list(range(1, n_z)) + [0]
+    order = list(range(2, n_z)) + [1, 0]
+    half = pos // 2
     totals = {}
 
-    def layer_of(step):
-        return lax.rem(z + order[step], n_z)
-
     def multiply(step):
-        layer = layer_of(step)
-        for half in range(2):
-            group = layer * CORES + (1 - core if half == 0 else core)
-            weight = column_of(meta_r[group, pl.ds(sp, 1), :], pos)[:, :1]
-            start = pl.multiple_of((group - layer * CORES) * pos, pos)
-            middle = mid_v[layer, pl.ds(start, pos), :]
-            for b in range(n_tp):
-                term = dot(middle, down_w[b]) * weight
-                if half == 0:
-                    pr_s[step, b] = term.astype(BF16)
-                else:
-                    acc_v[step % 2, b] = term
-            if half == 0:
-                send(pr_s.at[step], pr_r.at[step], pr_send.at[step], pr_recv.at[step], partner)
+        layer = layers[order[step]]
+        weight = jnp.concatenate([
+            column_of(meta_r[layer * CORES + i, pl.ds(sp, 1), :], pos)[:, :1]
+            for i in range(CORES)
+        ], axis=0)
+        middle = mid_v[layer]
+        for b in range(n_tp):
+            term = dot(middle, down_w[b]) * weight
+            lower, upper = term[:pos], term[pos:]
+            pr_s[step, b] = jnp.where(core == 0, upper, lower).astype(BF16)
+            acc_v[step % 3, b] = jnp.where(core == 0, lower, upper)
+        send(pr_s.at[step], pr_r.at[step], pr_send.at[step], pr_recv.at[step], partner)
+
+    def block_of(step, peer):
+        term = acc_v[step % 3, peer] + pr_r[step, peer].astype(F32)
+        if order[step] == 0:
+            cols = pl.ds(pl.multiple_of(peer * feats, feats), feats)
+            term = term + shared_v[:, cols]
+        return term
+
+    def cross(step):
+        arrived(pr_r.at[step], pr_recv.at[step])
+        if square:
+            rs_s[step, 2] = block_of(step, peers[2]).astype(BF16)
+            for b in range(2):
+                part = pl.ds(b * half, half)
+                send(rs_s.at[step, 2, part], rd_r.at[step, part], rs_send.at[step, 2 + b],
+                     rs_recv.at[step, 2 + b], {"tp": peers[b]})
+        rs_s[step, n_tp - 1] = block_of(step, tp).astype(BF16)
 
     def spread(step):
-        arrived(pr_r.at[step], pr_recv.at[step])
-        for b, peer in enumerate(peers + [tp]):
-            term = acc_v[step % 2, peer] + pr_r[step, peer].astype(F32)
-            if order[step] == 0:
-                cols = pl.ds(pl.multiple_of(peer * feats, feats), feats)
-                term = term + shared_v[:, cols]
+        if square:
+            for b in range(2):
+                part = pl.ds(b * half, half)
+                arrived(rd_r.at[step, part], rs_recv.at[step, 2 + b])
+        for b, peer in enumerate(near):
+            term = block_of(step, peer)
+            if square:
+                part = slice((1 - b) * half, (2 - b) * half)
+                extra = rd_r[step, part, :].astype(F32)
+                fixed = term[b * half:(b + 1) * half]
+                joined = [fixed, term[part] + extra]
+                term = jnp.concatenate(joined if b == 0 else joined[::-1], axis=0)
             rs_s[step, b] = term.astype(BF16)
-            if b < n_tp - 1:
-                send(rs_s.at[step, b], rs_r.at[step, b], rs_send.at[step, b],
-                     rs_recv.at[step, b], {"tp": peer})
+            send(rs_s.at[step, b], rs_r.at[step, b], rs_send.at[step, b],
+                 rs_recv.at[step, b], {"tp": peer})
 
     def gathered(step):
         total = rs_s[step, n_tp - 1].astype(F32)
-        for b in range(n_tp - 1):
+        for b in range(len(near)):
             arrived(rs_r.at[step, b], rs_recv.at[step, b])
             total = total + rs_r[step, b].astype(F32)
         d = order[step]
@@ -294,15 +327,12 @@
         else:
             zr_s[d] = total.astype(BF16)
             send(zr_s.at[d], zr_r.at[d], zr_send.at[d], zr_recv.at[d],
-                 {"sp": layer_of(step) * CORES + core})
-
-    for step in range(n_z + 2):
-        if step < n_z:
-            multiply(step)
-        if 0 <= step - 1 < n_z:
-            spread(step - 1)
-        if 0 <= step - 2 < n_z:
-            gathered(step - 2)
+                 {"sp": layers[d] * CORES + core})
+
+    for step in range(n_z + 3):
+        for lag, stage in enumerate((multiply, cross, spread, gathered)):
+            if 0 <= step - lag < n_z:
+                stage(step - lag)
 
     result = hidden_v[...] + totals[0]
     for d in range(1, n_z):
@@ -346,11 +376,12 @@
         pltpu.VMEM((n_sp, meta_rows, pos), F32),
         pltpu.VMEM((n_z, CORES * pos, hid), BF16),
         pltpu.VMEM((pos, width), F32),
-        pltpu.VMEM((2, n_tp, pos, feats), F32),
+        pltpu.VMEM((3, n_tp, pos, feats), F32),
         pltpu.VMEM((n_z, n_tp, pos, feats), BF16),
         pltpu.VMEM((n_z, n_tp, pos, feats), BF16),
         pltpu.VMEM((n_z, n_tp, pos, feats), BF16),
         pltpu.VMEM((n_z, n_tp, pos, feats), BF16),
+        pltpu.VMEM((n_z if n_tp == 4 else 1, pos, feats), BF16),
         pltpu.VMEM((n_z, pos, feats), BF16),
         pltpu.VMEM((n_z, pos, feats), BF16),
         dma((6,)), dma,
@@ -359,7 +390,7 @@
         dma((n_tp,)), dma((n_tp,)),
         dma((n_sp,)), dma((n_sp,)),
         dma((n_sp, n_tp)),
-        dma((n_z, n_tp)), dma((n_z,)), dma((n_z, n_tp)),
+        dma((n_z, n_tp)), dma((n_z,)), dma((n_z,)), dma((n_z, n_tp)),
         dma((n_tp, CHUNKS)), dma((n_tp, CHUNKS)),
         dma((n_z,)), dma((n_z,)),
         dma((n_z, n_tp)), dma((n_z, n_tp)),

time: 94.6 us -> 83.6 us (0.88)
  Pallas kernels: 90 us -> 79 us
    pallas_call x1, Pallas kernels: 90 us -> 79 us  [local(): pl.pallas_call(functools.partial(kernel, n_sp, n_tp), out_shape=jax.Shape...]
where the time goes in v2:
time: 83.6 us; the launch traced here: 83.4 us
  Pallas kernels  79 us (94%)
  local copies, waits for them, and re-layouts  4.39 us (5%)
    pallas_call x1, Pallas kernels, local(): pl.pallas_call(functools.partial(kernel, n_sp, n_tp), out_shape=jax.Shape...  79 us
    unnamed x3, local copies, waits for them, and re-layouts  4.39 us

profile of v2, /device:TPU:0, one launch (start us, length us, event | category | flops | bytes accessed | tf_op | source)
XLA Modules:
  0.0 83.4 jit_solution(5692830522095156710)
XLA Ops:
  0.0 1.4 %copy.18.routes = s32[128,4]{1,0:T(8,128)} copy(s32[128,4]{0,1:T(4,128)} %param.26) | data formatting | bytes 4096 | tf_op args[9]
  1.4 1.4 %copy.19.route_weight = f32[128,4]{1,0:T(8,128)} copy(f32[128,4]{0,1:T(4,128)} %param.27) | data formatting | bytes 4096 | tf_op args[10]
  2.8 79.0 %shard_map.163 = bf16[512,128]{1,0:T(8,128)(2,1)} custom-call(bf16[512,128]{1,0:T(8,128)(2,1)} %stream.1, bf16[256,128]{1,0:T(8,128)(2,1)} %values_in.1, bf16[256,128]{1,0:T(8,128)(2,1)} %in_gate.1, bf16[256,128]{1,0:T(8,128)(2,1)} %out_gate.1, s32[1,128]{1,0:T(1,128)} %bitcast.5, f32[3,256]{1,0:T(4,128)} %conv_taps.1, f32[1,256]{1,0:T(1,128)} %bitcast.4, ...), custom_call_target="tpu_custom_call" | custom-call | tf_op jit(solution)/shard_map/pallas_call | solution.py:399
  81.9 1.6 %copy.21 = bf16[512,128]{1,0:T(8,128)(2,1)} copy(bf16[512,128]{1,0:T(8,128)(2,1)} %shard_map.163) | data formatting | bytes 262144

commit v3 on v2

--- a/solution.py
+++ b/solution.py
@@ -129,11 +129,10 @@
     named = routes[...]
     weights = route_weight[...]
     meta_rows = meta_r.shape[1]
-    lane = lax.broadcasted_iota(jnp.int32, (pos, pos), 1)
-    table = jnp.zeros((pos, pos), F32)
-    for k in range(routes.shape[1]):
-        table = table + jnp.where(lane == named[:, k:k + 1], weights[:, k:k + 1], 0.0)
-    table = table.T[:meta_rows]
+    at_row = lax.broadcasted_iota(jnp.int32, (meta_rows, pos), 0)
+    table = jnp.zeros((meta_rows, pos), F32)
+    for k in range(routes.shape[0]):
+        table = table + jnp.where(at_row == named[k:k + 1, :], weights[k:k + 1, :], 0.0)
     taps = [column_of(conv_taps[j:j + 1, :], pos) for j in range(3)]
     stream_t = stream[...].astype(F32).T
 
@@ -186,7 +185,6 @@
         arrived(ss_r.at[b], ss_recv.at[b])
         row = row + ss_r[b]
     scale = lax.rsqrt(row[:1] / width + epsilon)
-    at_row = lax.broadcasted_iota(jnp.int32, (meta_rows, pos), 0)
     meta_r[sp] = jnp.where(at_row == meta_rows - 1, scale, table)
     for d in range(1, n_sp):
         send(meta_r.at[sp], meta_r.at[sp], meta_send.at[d], meta_recv.at[sp],
@@ -213,7 +211,7 @@
             send(block, block, xs_d.at[d], x_recv.at[sp, peers[2]],
                  {"sp": layers[d] * CORES + core})
     from_layer(1)
-    for chunk in (4, 5):
+    for chunk in range(4, CHUNKS):
         send_down(chunk)
 
     loads[1].wait()
@@ -231,12 +229,10 @@
 
     for d in range(2, n_z):
         from_layer(d)
-    for chunk in (6, 7):
-        send_down(chunk)
 
     loads[4].wait()
     loads[5].wait()
-    for d in range(n_z):
+    def widen(d):
         layer = layers[d]
         mine = layer * CORES + core
         other = layer * CORES + 1 - core
@@ -259,12 +255,15 @@
         ], axis=0)
         mid_v[layer] = (silu(gate * scales) * (upward * scales)).astype(BF16)
 
+    widen(0)
+    if n_z > 1:
+        widen(1)
     own_down.wait()
     for peer in peers:
         for chunk in range(CHUNKS):
             arrived(down_w.at[peer, pl.ds(chunk * rows, rows), :], wd_recv.at[peer, chunk])
 
-    order = list(range(2, n_z)) + [1, 0]
+    order = list(range(1, n_z)) + [0]
     half = pos // 2
     totals = {}
 
@@ -329,8 +328,12 @@
             send(zr_s.at[d], zr_r.at[d], zr_send.at[d], zr_recv.at[d],
                  {"sp": layers[d] * CORES + core})
 
-    for step in range(n_z + 3):
-        for lag, stage in enumerate((multiply, cross, spread, gathered)):
+    for step in range(n_z + 2):
+        if step < n_z:
+            multiply(step)
+            if step + 2 < n_z:
+                widen(step + 2)
+        for lag, stage in enumerate((cross, spread, gathered)):
             if 0 <= step - lag < n_z:
                 stage(step - lag)
 
@@ -407,8 +410,8 @@
         ),
     )(
         stream, values_in, in_gate, out_gate, documents.reshape(1, pos), conv_taps,
-        head_gain.reshape(1, chans), mix_weight, norm_gain.reshape(1, feats), routes,
-        route_weight, expert_gate, expert_up, expert_down, shared_gate, shared_up, shared_down,
+        head_gain.reshape(1, chans), mix_weight, norm_gain.reshape(1, feats), routes.T,
+        route_weight.T, expert_gate, expert_up, expert_down, shared_gate, shared_up, shared_down,
     )
 
 

time: 83.6 us -> 80.9 us (0.968)
  local copies, waits for them, and re-layouts: 4.39 us -> 1.57 us
    unnamed x3 -> x1, local copies, waits for them, and re-layouts: 4.39 us -> 1.57 us
where the time goes in v3:
time: 80.9 us; the launch traced here: 80.7 us
  Pallas kernels  79.2 us (98%)
  local copies, waits for them, and re-layouts  1.57 us (2%)
    pallas_call x1, Pallas kernels, local(): pl.pallas_call(functools.partial(kernel, n_sp, n_tp), out_shape=jax.Shape...  79.2 us

profile of v3, /device:TPU:0, one launch (start us, length us, event | category | flops | bytes accessed | tf_op | source)
XLA Modules:
  0.0 80.7 jit_solution(13238692475989368464)
XLA Ops:
  0.0 79.2 %shard_map.163 = bf16[512,128]{1,0:T(8,128)(2,1)} custom-call(bf16[512,128]{1,0:T(8,128)(2,1)} %stream.1, bf16[256,128]{1,0:T(8,128)(2,1)} %values_in.1, bf16[256,128]{1,0:T(8,128)(2,1)} %in_gate.1, bf16[256,128]{1,0:T(8,128)(2,1)} %out_gate.1, s32[1,128]{1,0:T(1,128)} %bitcast.9, f32[3,256]{1,0:T(4,128)} %conv_taps.1, f32[1,256]{1,0:T(1,128)} %bitcast.8, ...), custom_call_target="tpu_custom_call" | custom-call | tf_op jit(solution)/shard_map/pallas_call | solution.py:402
  79.2 1.6 %copy.19 = bf16[512,128]{1,0:T(8,128)(2,1)} copy(bf16[512,128]{1,0:T(8,128)(2,1)} %shard_map.163) | data formatting | bytes 262144

commit v4 on v3

--- a/solution.py
+++ b/solution.py
@@ -47,10 +47,10 @@
     out,
     mix_w, gate_w, up_w, sgate_w, sup_w, sdown_w, down_w,
     tail_s, prev_r, prev_docs, mix_s, mix_r, hidden_v, x_all, ss_s, ss_r, meta_r,
-    mid_v, shared_v, acc_v, pr_s, pr_r, rs_s, rs_r, rd_r, zr_s, zr_r,
+    mid_v, shared_v, acc_v, pr_s, pr_r, rs_s, rs_r, rd_r, rz_r, zr_s, zr_r,
     load_sem, local_sem, halo_send, halo_recv, mix_send, mix_recv, ss_send, ss_recv,
-    meta_send, meta_recv, x_recv, xs_tp, xs_z, xs_d, xs_p, wd_send, wd_recv,
-    pr_send, pr_recv, rs_send, rs_recv, zr_send, zr_recv,
+    meta_send, meta_recv, x_recv, xs_tp, xs_z, xs_d, xs_n, xs_p, wd_send, wd_recv,
+    pr_send, pr_recv, rs_send, rs_recv, zr_send, zr_recv, rz_send, rz_recv,
 ):
     sp = lax.axis_index("sp")
     tp = lax.axis_index("tp")
@@ -63,7 +63,7 @@
     hid = gate_w.shape[1]
     partner = {"sp": z * CORES + 1 - core}
     peers = [flipped(tp, d) for d in range(1, n_tp)]
-    square = n_tp == 4
+    square = n_tp == 4 and n_z > 1
     near = peers[:2] if square else peers
     layers = [flipped(z, d) for d in range(n_z)]
     pending = []
@@ -199,12 +199,16 @@
         group = layers[d] * CORES + core
         block = x_all.at[group, tp]
         arrived(block, x_recv.at[group, tp])
-        for b, peer in enumerate(near):
+        for b, peer in enumerate([] if square and d == 1 else near):
             send(block, block, xs_tp.at[d, b], x_recv.at[group, tp], {"tp": peer})
         send(block, block, xs_p.at[d, 0], x_recv.at[group, tp], partner)
 
     for b in range(n_tp - 1):
         to_partner(0, b, sp)
+        if square and b < 2:
+            block = x_all.at[sp, peers[b]]
+            send(block, block, xs_n.at[b], x_recv.at[sp, peers[b]],
+                 {"sp": layers[1] * CORES + core})
     if square:
         block = x_all.at[sp, peers[2]]
         for d in range(1, n_z):
@@ -265,6 +269,10 @@
 
     order = list(range(1, n_z)) + [0]
     half = pos // 2
+
+    def direct(step):
+        return square and order[step] == 1
+
     totals = {}
 
     def multiply(step):
@@ -286,10 +294,19 @@
         if order[step] == 0:
             cols = pl.ds(pl.multiple_of(peer * feats, feats), feats)
             term = term + shared_v[:, cols]
+            if square:
+                term = term + rz_r[peer].astype(F32)
         return term
 
     def cross(step):
         arrived(pr_r.at[step], pr_recv.at[step])
+        if direct(step):
+            for b in range(n_tp):
+                rs_s[step, b] = block_of(step, b).astype(BF16)
+            send(rs_s.at[step], rz_r, rz_send, rz_recv, {"sp": layers[1] * CORES + core})
+            return
+        if square and order[step] == 0:
+            arrived(rz_r, rz_recv)
         if square:
             rs_s[step, 2] = block_of(step, peers[2]).astype(BF16)
             for b in range(2):
@@ -299,6 +316,8 @@
         rs_s[step, n_tp - 1] = block_of(step, tp).astype(BF16)
 
     def spread(step):
+        if direct(step):
+            return
         if square:
             for b in range(2):
                 part = pl.ds(b * half, half)
@@ -316,6 +335,8 @@
                  rs_recv.at[step, b], {"tp": peer})
 
     def gathered(step):
+        if direct(step):
+            return
         total = rs_s[step, n_tp - 1].astype(F32)
         for b in range(len(near)):
             arrived(rs_r.at[step, b], rs_recv.at[step, b])
@@ -338,7 +359,7 @@
                 stage(step - lag)
 
     result = hidden_v[...] + totals[0]
-    for d in range(1, n_z):
+    for d in range(2 if square else 1, n_z):
         arrived(zr_r.at[d], zr_recv.at[d])
         result = result + zr_r[d].astype(F32)
     out[...] = result.T.astype(BF16)
@@ -385,6 +406,7 @@
         pltpu.VMEM((n_z, n_tp, pos, feats), BF16),
         pltpu.VMEM((n_z, n_tp, pos, feats), BF16),
         pltpu.VMEM((n_z if n_tp == 4 else 1, pos, feats), BF16),
+        pltpu.VMEM((n_tp if n_tp == 4 else 1, pos, feats), BF16),
         pltpu.VMEM((n_z, pos, feats), BF16),
         pltpu.VMEM((n_z, pos, feats), BF16),
         dma((6,)), dma,
@@ -393,11 +415,12 @@
         dma((n_tp,)), dma((n_tp,)),
         dma((n_sp,)), dma((n_sp,)),
         dma((n_sp, n_tp)),
-        dma((n_z, n_tp)), dma((n_z,)), dma((n_z,)), dma((n_z, n_tp)),
+        dma((n_z, n_tp)), dma((n_z,)), dma((n_z,)), dma((n_tp,)), dma((n_z, n_tp)),
         dma((n_tp, CHUNKS)), dma((n_tp, CHUNKS)),
         dma((n_z,)), dma((n_z,)),
         dma((n_z, n_tp)), dma((n_z, n_tp)),
         dma((n_z,)), dma((n_z,)),
+        dma, dma,
     ]
     return pl.pallas_call(
         functools.partial(kernel, n_sp, n_tp),

time: 80.9 us -> 80.7 us (level)
  no operation moved by 1% of the time
where the time goes in v4:
time: 80.7 us; the launch traced here: 80.6 us
  Pallas kernels  79 us (98%)
  local copies, waits for them, and re-layouts  1.57 us (2%)
    pallas_call x1, Pallas kernels, local(): pl.pallas_call(functools.partial(kernel, n_sp, n_tp), out_shape=jax.Shape...  79 us

profile of v4, /device:TPU:0, one launch (start us, length us, event | category | flops | bytes accessed | tf_op | source)
XLA Modules:
  0.0 80.6 jit_solution(1558279368504082582)
XLA Ops:
  0.0 79.0 %shard_map.163 = bf16[512,128]{1,0:T(8,128)(2,1)} custom-call(bf16[512,128]{1,0:T(8,128)(2,1)} %stream.1, bf16[256,128]{1,0:T(8,128)(2,1)} %values_in.1, bf16[256,128]{1,0:T(8,128)(2,1)} %in_gate.1, bf16[256,128]{1,0:T(8,128)(2,1)} %out_gate.1, s32[1,128]{1,0:T(1,128)} %bitcast.9, f32[3,256]{1,0:T(4,128)} %conv_taps.1, f32[1,256]{1,0:T(1,128)} %bitcast.8, ...), custom_call_target="tpu_custom_call" | custom-call | tf_op jit(solution)/shard_map/pallas_call | solution.py:425
  79.0 1.6 %copy.19 = bf16[512,128]{1,0:T(8,128)(2,1)} copy(bf16[512,128]{1,0:T(8,128)(2,1)} %shard_map.163) | data formatting | bytes 262144

commit v5 on v4

--- a/solution.py
+++ b/solution.py
@@ -11,6 +11,8 @@
 CORES = 2
 CHUNKS = 8
 SUB = 8
+PLAN = (1, 1, 1, 5, 0)
+ALONG_Z = (1, 2)
 epsilon = 1e-06
 MESH = pl.DeviceIdType.MESH
 F32 = jnp.float32
@@ -65,6 +67,7 @@
     peers = [flipped(tp, d) for d in range(1, n_tp)]
     square = n_tp == 4 and n_z > 1
     near = peers[:2] if square else peers
+    along_z = [d for d in ALONG_Z if d < n_z] if square else []
     layers = [flipped(z, d) for d in range(n_z)]
     pending = []
 
@@ -108,6 +111,13 @@
 
     rows = hid // CHUNKS
 
+    sent_chunks = []
+
+    def send_chunks(stage):
+        for _ in range(PLAN[stage]):
+            send_down(len(sent_chunks))
+            sent_chunks.append(stage)
+
     def send_down(chunk):
         for d, peer in enumerate(peers):
             start = pl.multiple_of(peer * hid + chunk * rows, rows)
@@ -117,8 +127,7 @@
                 wd_send.at[d, chunk], wd_recv.at[tp, chunk], {"tp": peer},
             )
 
-    for chunk in (0, 1):
-        send_down(chunk)
+    send_chunks(0)
     own_down = pltpu.make_async_copy(
         expert_down.at[0, pl.ds(pl.multiple_of(tp * hid, hid), hid), :], down_w.at[tp], local_sem
     )
@@ -160,7 +169,7 @@
         mix_s[b] = dot(heads_t, mix_w[:, cols]).astype(BF16)
         if b < n_tp - 1:
             send(mix_s.at[b], mix_r.at[b], mix_send.at[b], mix_recv.at[b], {"tp": peer})
-    send_down(2)
+    send_chunks(1)
 
     hidden = stream_t + mix_s[n_tp - 1].astype(F32)
     for b in range(n_tp - 1):
@@ -180,7 +189,7 @@
     ss_s[...] = row
     for b, peer in enumerate(peers):
         send(ss_s, ss_r.at[b], ss_send.at[b], ss_recv.at[b], {"tp": peer})
-    send_down(3)
+    send_chunks(2)
     for b in range(n_tp - 1):
         arrived(ss_r.at[b], ss_recv.at[b])
         row = row + ss_r[b]
@@ -199,7 +208,7 @@
         group = layers[d] * CORES + core
         block = x_all.at[group, tp]
         arrived(block, x_recv.at[group, tp])
-        for b, peer in enumerate([] if square and d == 1 else near):
+        for b, peer in enumerate([] if square and d == 1 else (near if d in along_z else peers)):
             send(block, block, xs_tp.at[d, b], x_recv.at[group, tp], {"tp": peer})
         send(block, block, xs_p.at[d, 0], x_recv.at[group, tp], partner)
 
@@ -211,12 +220,11 @@
                  {"sp": layers[1] * CORES + core})
     if square:
         block = x_all.at[sp, peers[2]]
-        for d in range(1, n_z):
+        for d in along_z:
             send(block, block, xs_d.at[d], x_recv.at[sp, peers[2]],
                  {"sp": layers[d] * CORES + core})
     from_layer(1)
-    for chunk in range(4, CHUNKS):
-        send_down(chunk)
+    send_chunks(3)
 
     loads[1].wait()
     loads[2].wait()
@@ -233,6 +241,7 @@
 
     for d in range(2, n_z):
         from_layer(d)
+    send_chunks(4)
 
     loads[4].wait()
     loads[5].wait()

time: 80.7 us -> 78.3 us (0.970)
  Pallas kernels: 79 us -> 76 us
    pallas_call x1, Pallas kernels: 79 us -> 76 us  [local(): pl.pallas_call(functools.partial(kernel, n_sp, n_tp), out_shape=jax.Shape...]
where the time goes in v5:
time: 78.3 us; the launch traced here: 77.6 us
  Pallas kernels  76 us (97%)
  local copies, waits for them, and re-layouts  1.57 us (2%)
    pallas_call x1, Pallas kernels, local(): pl.pallas_call(functools.partial(kernel, n_sp, n_tp), out_shape=jax.Shape...  76 us
    unnamed x1, local copies, waits for them, and re-layouts  1.57 us

profile of v5, /device:TPU:0, one launch (start us, length us, event | category | flops | bytes accessed | tf_op | source)
XLA Modules:
  0.0 77.6 jit_solution(14276409884369765665)
XLA Ops:
  0.0 76.0 %shard_map.163 = bf16[512,128]{1,0:T(8,128)(2,1)} custom-call(bf16[512,128]{1,0:T(8,128)(2,1)} %stream.1, bf16[256,128]{1,0:T(8,128)(2,1)} %values_in.1, bf16[256,128]{1,0:T(8,128)(2,1)} %in_gate.1, bf16[256,128]{1,0:T(8,128)(2,1)} %out_gate.1, s32[1,128]{1,0:T(1,128)} %bitcast.9, f32[3,256]{1,0:T(4,128)} %conv_taps.1, f32[1,256]{1,0:T(1,128)} %bitcast.8, ...), custom_call_target="tpu_custom_call" | custom-call | tf_op jit(solution)/shard_map/pallas_call | solution.py:434
  76.0 1.6 %copy.19 = bf16[512,128]{1,0:T(8,128)(2,1)} copy(bf16[512,128]{1,0:T(8,128)(2,1)} %shard_map.163) | data formatting | bytes 262144
